TPU v7x, 32 devices: a whole 2x2x4 slice. The times are simulated.
32 devices in a mesh: kv: 8 (over z, y), tp: 4 (over x, core).
Axes of the slice: x: 2, y: 2, z: 4, core: 2. Of those that a mesh axis runs over, the one named last changes fastest.
Arguments:
- tokens: bfloat16 [16, 3072], P('kv', 'tp'), may hold values from -15 to 15
- associative_state: float32 [16, 16, 128, 128], P('kv', 'tp'), may hold values from -2 to 2
- sudden_extra_decay: float32 [16, 16], P('kv', 'tp'), may hold values from -0.7 to 0
- head_decay_speed: float32 [16], P('tp'), may hold values from 0.05 to 2
- opening_norm_gain: float32 [3072], P('tp'), may hold values from 0.1 to 1.9
- opening_gate_weight: bfloat16 [3072, 8448], P('tp', 'kv'), may hold values from -0.109375 to 0.109375
- opening_up_weight: bfloat16 [3072, 8448], P('tp', 'kv'), may hold values from -0.109375 to 0.109375
- opening_down_weight: bfloat16 [8448, 3072], P('kv', 'tp'), may hold values from -0.25 to 0.25
- mixer_norm_gain: float32 [3072], P('tp'), may hold values from 0.1 to 1.9
- query_matrix: bfloat16 [3072, 2048], P('tp'), may hold values from -0.109375 to 0.109375
- key_matrix: bfloat16 [3072, 2048], P('tp'), may hold values from -0.109375 to 0.109375
- value_matrix: bfloat16 [3072, 2048], P('tp'), may hold values from -0.109375 to 0.109375
- output_gate_matrix: bfloat16 [3072, 2048], P('tp'), may hold values from -0.109375 to 0.109375
- strength_weight: bfloat16 [3072, 16], P('tp'), may hold values from -0.109375 to 0.109375
- decay_matrix: bfloat16 [3072, 16], P('tp'), may hold values from -0.109375 to 0.109375
- head_read_gain: float32 [128], replicated, may hold values from 0.1 to 1.9
- output_matrix: bfloat16 [2048, 3072], P('tp'), may hold values from -0.125 to 0.125
- closing_norm_gain: float32 [3072], P('tp'), may hold values from 0.1 to 1.9
- closing_gate_weight: bfloat16 [3072, 8448], P('tp', 'kv'), may hold values from -0.109375 to 0.109375
- closing_up_weight: bfloat16 [3072, 8448], P('tp', 'kv'), may hold values from -0.109375 to 0.109375
- closing_down_weight: bfloat16 [8448, 3072], P('kv', 'tp'), may hold values from -0.25 to 0.25
Outputs:
- layer_out: bfloat16 [16, 3072], P('kv', 'tp')
- memory_new: float32 [16, 16, 128, 128], P('kv', 'tp')
All inputs are finite; a program needn't handle non-finite values.
Results may differ from a plain program's by a relative error of at most 0.023.
Values may be sent and summed in bfloat16 or wider, within the bound.
A program may use at most 64 MiB of HBM per device.

v0:
```python
import jax
import jax.numpy as jnp
from jax import lax
from jax.sharding import PartitionSpec as P

norm_eps = 1e-06


def feed_forward(resid, rows_in, gain, gate_proj, lift_proj, down_proj):
    model_width = gain.shape[0] * lax.axis_size("tp")
    gathered = lax.all_gather(rows_in, "kv", axis=0, tiled=True)
    values = gathered.astype(jnp.float32)
    scaled = (values * gain).astype(jnp.bfloat16)
    gate_part = jnp.dot(scaled, gate_proj, preferred_element_type=jnp.float32)
    lift_part = jnp.dot(scaled, lift_proj, preferred_element_type=jnp.float32)
    square = jnp.sum(values * values, axis=1)
    gate_sum, lift_sum, square_sum = (
        lax.psum(gate_part.astype(jnp.bfloat16), "tp").astype(jnp.float32),
        lax.psum(lift_part.astype(jnp.bfloat16), "tp").astype(jnp.float32),
        lax.psum(square.astype(jnp.bfloat16), "tp").astype(jnp.float32),
    )
    scale_of_norm = lax.rsqrt(square_sum / model_width + norm_eps)[:, None]
    hidden = (jax.nn.silu(scale_of_norm * gate_sum) * (scale_of_norm * lift_sum)).astype(
        jnp.bfloat16
    )
    down_part = jnp.dot(hidden, down_proj, preferred_element_type=jnp.float32)
    whole_sum = lax.psum(down_part, "kv")
    row_count = resid.shape[0]
    own_rows = lax.dynamic_slice_in_dim(whole_sum, lax.axis_index("kv") * row_count, row_count, 0)
    return resid + 0.5 * own_rows.astype(jnp.bfloat16).astype(jnp.float32)


def unit_norm(values):
    return values * lax.rsqrt(jnp.sum(values * values, axis=-1, keepdims=True) + 1e-12)


def body(
    tokens,
    associative_state,
    sudden_extra_decay,
    head_decay_speed,
    opening_norm_gain,
    opening_gate_weight,
    opening_up_weight,
    opening_down_weight,
    mixer_norm_gain,
    query_matrix,
    key_matrix,
    value_matrix,
    output_gate_matrix,
    strength_weight,
    decay_matrix,
    head_read_gain,
    output_matrix,
    closing_norm_gain,
    closing_gate_weight,
    closing_up_weight,
    closing_down_weight,
):
    model_width = opening_norm_gain.shape[0] * lax.axis_size("tp")
    first = feed_forward(
        tokens.astype(jnp.float32),
        tokens,
        opening_norm_gain,
        opening_gate_weight,
        opening_up_weight,
        opening_down_weight,
    )
    square_sum = lax.psum(jnp.sum(first * first, axis=1), "tp")
    scale_of_norm = lax.rsqrt(square_sum / model_width + norm_eps)[:, None]
    mixer_input = (first * mixer_norm_gain).astype(jnp.bfloat16)
    partials = tuple(
        (
            jnp.dot(mixer_input, weight, preferred_element_type=jnp.float32).astype(jnp.bfloat16)
            for weight in (
                query_matrix,
                key_matrix,
                value_matrix,
                output_gate_matrix,
                strength_weight,
                decay_matrix,
            )
        )
    )
    query_sum, key_sum, value_sum, gate_sum, beta_sum, decay_total = (
        lax.psum_scatter(partials[0], "tp", scatter_dimension=1, tiled=True).astype(jnp.float32),
        lax.psum_scatter(partials[1], "tp", scatter_dimension=1, tiled=True).astype(jnp.float32),
        lax.psum_scatter(partials[2], "tp", scatter_dimension=1, tiled=True).astype(jnp.float32),
        lax.psum_scatter(partials[3], "tp", scatter_dimension=1, tiled=True).astype(jnp.float32),
        lax.psum_scatter(partials[4], "tp", scatter_dimension=1, tiled=True).astype(jnp.float32),
        lax.psum_scatter(partials[5], "tp", scatter_dimension=1, tiled=True).astype(jnp.float32),
    )
    row_count = query_sum.shape[0]
    head_count = head_decay_speed.shape[0]
    head_size = head_read_gain.shape[0]

    def split_heads(values):
        return (scale_of_norm * values).reshape(row_count, head_count, head_size)

    query_vec = unit_norm(split_heads(query_sum)) * head_size ** (-0.5)
    key_vec = unit_norm(split_heads(key_sum))
    value_vec = split_heads(value_sum)
    gate_vec = split_heads(gate_sum)
    beta = jax.nn.sigmoid(scale_of_norm * beta_sum)
    decay_logarithm = (
        -head_decay_speed * jax.nn.softplus(scale_of_norm * decay_total) + sudden_extra_decay
    )
    kept = jnp.exp(decay_logarithm)[:, :, None, None]
    recall = jnp.einsum(
        "bhk,bhkv->bhv", key_vec, associative_state, precision=lax.Precision.HIGHEST
    )
    written = (beta[:, :, None] * key_vec)[:, :, :, None]
    memory_new = (
        kept * (associative_state - written * recall[:, :, None, :])
        + written * value_vec[:, :, None, :]
    )
    read_out = jnp.einsum("bhk,bhkv->bhv", query_vec, memory_new, precision=lax.Precision.HIGHEST)
    normed = read_out * lax.rsqrt(jnp.mean(read_out * read_out, axis=-1, keepdims=True) + norm_eps)
    normed = normed * head_read_gain * jax.nn.silu(gate_vec)
    mix_out = normed.reshape(row_count, head_count * head_size).astype(jnp.bfloat16)
    out_part = jnp.dot(mix_out, output_matrix, preferred_element_type=jnp.float32).astype(
        jnp.bfloat16
    )
    mixed = lax.psum_scatter(out_part, "tp", scatter_dimension=1, tiled=True).astype(jnp.float32)
    second = first + mixed.astype(jnp.bfloat16).astype(jnp.float32)
    final = feed_forward(
        second,
        second.astype(jnp.bfloat16),
        closing_norm_gain,
        closing_gate_weight,
        closing_up_weight,
        closing_down_weight,
    )
    return (final.astype(jnp.bfloat16), memory_new)


def solution(mesh):
    placed = (
        P("kv", "tp"),
        P("kv", "tp", None, None),
        P("kv", "tp"),
        P("tp"),
        P("tp"),
        P("tp", "kv"),
        P("tp", "kv"),
        P("kv", "tp"),
        P("tp"),
        P("tp", None),
        P("tp", None),
        P("tp", None),
        P("tp", None),
        P("tp", None),
        P("tp", None),
        P(),
        P("tp", None),
        P("tp"),
        P("tp", "kv"),
        P("tp", "kv"),
        P("kv", "tp"),
    )
    return jax.shard_map(
        body,
        mesh=mesh,
        in_specs=placed,
        out_specs=(P("kv", "tp"), P("kv", "tp", None, None)),
        check_vma=False,
    )
```

profile of v0, /device:TPU:0, one launch (start us, length us, event | category | flops | bytes accessed | tf_op | source)
XLA Modules:
  0.0 359.4 jit_solution(2355526956701864364)
XLA Ops:
  7.2 32.6 %all-gather = bf16[8,2,768]{2,1,0:T(2,128)(2,1)S(1)} all-gather(bf16[1,2,768]{2,1,0:T(2,128)(2,1)} %bitcast.66), channel_id=1, replica_groups=mesh['kv'=8,'tp'=4] {'kv'}, dimensions={0}, use_global_device_ids=true | all-gather | bytes 27648 | tf_op jit(solution)/shard_map/all_gather | solution.py:11
  39.9 0.6 multiply_reduce_fusion.1
  40.5 2.6 convolution_convert_fusion.3
  43.2 1.2 convolution_convert_fusion.4
  44.4 0.6 dynamic-slice
  45.7 29.5 %all-reduce.10.cloned.1.call-done = (bf16[16,1056]{1,0:T(8,128)(2,1)}, bf16[16,1056]{1,0:T(8,128)(2,1)}, bf16[16]{0:T(256)(128)(2,1)}) async-done(((bf16[16,1056]{1,0:T(8,128)(2,1)}, bf16[16,1056]{1,0:T(8,128)(2,1)}, bf16[16]{0:T(256)(128)(2,1)}), (bf16[16,1056]{1,0:T(8,128)(2,1)}, bf16[16,1056]{1,0:T(8,128)(2,1)}, bf16[16]{0:T(256)(128)(2,1)})) %all-reduce.10.cloned.1.call-update) | async-done | bytes 67632 | tf_op jit(solution)/shard_map/psum | solution.py:19
  75.2 0.7 add_rsqrt_fusion.5
  75.9 1.9 fusion
  77.7 37.9 %psum.66 = bf16[16,768]{1,0:T(8,128)(2,1)S(1)} all-reduce(f32[16,768]{1,0:T(8,128)S(1)} %fusion), channel_id=1, replica_groups=mesh['kv'=8,'tp'=4] {'kv'}, use_global_device_ids=true, to_apply=%region_4.5 | all-reduce | flops 12288 | bytes 73728 | tf_op jit(solution)/shard_map/psum | solution.py:27
  115.7 0.1 multiply_reduce_fusion.2
  115.8 2.6 convolution_convert_fusion.5
  118.4 0.1 copy-done.1
  118.5 0.5 convolution_convert_fusion.6
  119.0 1.4 copy-done.2
  120.4 0.5 convolution_convert_fusion.8
  120.9 1.1 copy.27
  122.1 2.4 convolution_convert_fusion.7
  124.5 1.1 copy.31
  125.6 0.1 convolution_convert_fusion.9
  125.8 1.1 copy.33
  126.9 0.1 convolution_convert_fusion.10
  127.0 5.6 %psum.67 = f32[2]{0:T(128)S(1)} all-reduce(f32[2]{0:T(128)S(1)} %get-tuple-element.12), channel_id=1, replica_groups=mesh['kv'=8,'tp'=4] {'tp'}, use_global_device_ids=true, to_apply=%region_6.7 | all-reduce | flops 2 | bytes 16 | tf_op jit(solution)/shard_map/psum | solution.py:69
  132.7 1.1 copy.35
  133.8 7.8 %all-reduce.3 = (bf16[2,16]{1,0:T(2,128)(2,1)S(1)}, bf16[2,16]{1,0:T(2,128)(2,1)S(1)}) all-reduce(bf16[2,16]{1,0:T(2,128)(2,1)S(1)} %convolution_convert_fusion.9, bf16[2,16]{1,0:T(2,128)(2,1)S(1)} %convolution_convert_fusion.10), channel_id=4, replica_groups=mesh['kv'=8,'tp'=4] {'tp'}, use_global_device_ids=true, to_apply=%region_10.11.clone | all-reduce | flops 64 | bytes 256
  141.7 1.0 copy.28
  142.7 23.7 %reduce-scatter.20.cloned.1.call-done = bf16[512,2]{1,0:T(8,128)(2,1)} async-done(((bf16[2048,2]{1,0:T(8,128)(2,1)}), bf16[512,2]{1,0:T(8,128)(2,1)}) %reduce-scatter.20.cloned.1.call-update) | async-done | bytes 2064
  166.4 1.0 copy.32
  167.4 23.0 %reduce-scatter.22.cloned.1.call-done = bf16[512,2]{1,0:T(8,128)(2,1)} async-done(((bf16[2048,2]{1,0:T(8,128)(2,1)}), bf16[512,2]{1,0:T(8,128)(2,1)}) %reduce-scatter.22.cloned.1.call-update) | async-done | bytes 2064
  190.4 1.0 copy.34
  191.4 23.0 %reduce-scatter.24.cloned.1.call-done = bf16[512,2]{1,0:T(8,128)(2,1)} async-done(((bf16[2048,2]{1,0:T(8,128)(2,1)}), bf16[512,2]{1,0:T(8,128)(2,1)}) %reduce-scatter.24.cloned.1.call-update) | async-done | bytes 2064
  214.4 1.0 copy.36
  216.0 1.6 fusion.18
  217.6 1.3 multiply_add_fusion
  218.9 0.8 copy-done.3
  219.7 0.5 fusion.19
  220.4 0.5 convolution_convert_fusion
  220.9 1.2 copy.37
  222.2 23.3 %reduce-scatter.26.cloned.1.call-done = bf16[768,2]{1,0:T(8,128)(2,1)} async-done(((bf16[3072,2]{1,0:T(8,128)(2,1)}), bf16[768,2]{1,0:T(8,128)(2,1)}) %reduce-scatter.26.cloned.1.call-update) | async-done | bytes 3088
  245.5 1.0 copy.38
  246.6 30.6 %all-gather.1 = bf16[8,2,768]{2,1,0:T(2,128)(2,1)S(1)} all-gather(bf16[1,2,768]{2,1,0:T(2,128)(2,1)S(1)} %fusion.9), channel_id=1, replica_groups=mesh['kv'=8,'tp'=4] {'kv'}, dimensions={0}, use_global_device_ids=true | all-gather | bytes 27648 | tf_op jit(solution)/shard_map/all_gather | solution.py:11
  277.2 0.6 multiply_reduce_fusion
  277.9 2.6 convolution_convert_fusion.1
  280.4 1.2 convolution_convert_fusion.2
  281.6 29.9 %all-reduce.8.cloned.1.call-done = (bf16[16,1056]{1,0:T(8,128)(2,1)}, bf16[16,1056]{1,0:T(8,128)(2,1)}, bf16[16]{0:T(256)(128)(2,1)}) async-done(((bf16[16,1056]{1,0:T(8,128)(2,1)}, bf16[16,1056]{1,0:T(8,128)(2,1)}, bf16[16]{0:T(256)(128)(2,1)}), (bf16[16,1056]{1,0:T(8,128)(2,1)}, bf16[16,1056]{1,0:T(8,128)(2,1)}, bf16[16]{0:T(256)(128)(2,1)})) %all-reduce.8.cloned.1.call-update) | async-done | bytes 67632 | tf_op jit(solution)/shard_map/psum | solution.py:19
  311.5 0.7 add_rsqrt_fusion.3
  312.2 1.9 fusion.1
  314.1 37.9 %psum.71 = bf16[16,768]{1,0:T(8,128)(2,1)S(1)} all-reduce(f32[16,768]{1,0:T(8,128)S(1)} %fusion.1), channel_id=1, replica_groups=mesh['kv'=8,'tp'=4] {'kv'}, use_global_device_ids=true, to_apply=%region_21.22 | all-reduce | flops 12288 | bytes 73728 | tf_op jit(solution)/shard_map/psum | solution.py:27
  352.0 0.6 add_convert_fusion
  (63 shorter events, 1.3 us)
Async XLA Ops:
  7.2 213.2 %copy-start = (bf16[512,3072]{1,0:T(8,128)(2,1)S(1)}, bf16[512,3072]{1,0:T(8,128)(2,1)}, u32[]{:S(2)}) copy-start(bf16[512,3072]{1,0:T(8,128)(2,1)} %param.37) | copy-start | bytes 9437188
  7.2 36.0 %copy-start.7 = (f32[768]{0:T(1024)S(1)}, f32[768]{0:T(1024)}, u32[]{:S(2)}) copy-start(f32[768]{0:T(1024)} %param.25) | copy-start | bytes 9220
  7.2 68.0 %all-reduce.10.cloned.1.call-start = ((), (), s32[]{:S(2)}) async-start(), calls=%async_computation.11 | async-start | bytes 148480 | tf_op jit(solution)/shard_map/psum | solution.py:19
  39.9 3.3 copy-start.4
  40.5 3.9 %copy-start.14 = (f32[4]{0:T(128)S(1)}, f32[4]{0:T(128)}, u32[]{:S(2)}) copy-start(f32[4]{0:T(128)} %param.24) | copy-start | bytes 52
  40.5 3.9 %copy-start.15 = (u32[32]{0:T(128)S(1)}, u32[32]{0:T(128)}, u32[]{:S(2)}) copy-start(u32[32]{0:T(128)} %constant.47) | copy-start | bytes 388
  43.1 72.5 %copy-start.6 = (bf16[2,768]{1,0:T(2,128)(2,1)S(1)}, bf16[2,768]{1,0:T(2,128)(2,1)}, u32[]{:S(2)}) copy-start(bf16[2,768]{1,0:T(2,128)(2,1)} %param.21) | copy-start | bytes 9220
  43.1 72.5 %copy-start.9 = (f32[768]{0:T(1024)S(1)}, f32[768]{0:T(1024)}, u32[]{:S(2)}) copy-start(f32[768]{0:T(1024)} %param.29) | copy-start | bytes 9220
  44.3 97.4 %reduce-scatter.18.cloned.1.call-start = ((), (), s32[]{:S(2)}) async-start(), calls=%async_computation.5 | async-start | bytes 655360
  115.7 2.8 copy-start.1
  118.5 1.9 copy-start.2
  122.0 3.6 %copy-start.12 = (bf16[768,16]{0,1:T(8,128)(2,1)S(1)}, bf16[768,16]{0,1:T(8,128)(2,1)}, u32[]{:S(2)}) copy-start(bf16[768,16]{0,1:T(8,128)(2,1)} %param.34) | copy-start | bytes 73732
  122.0 44.3 %reduce-scatter.20.cloned.1.call-start = ((), (), s32[]{:S(2)}) async-start(), calls=%async_computation.6 | async-start | bytes 655360
  124.5 2.4 copy-start.13
  125.6 90.3 %copy-start.10 = (f32[2,4]{1,0:T(2,128)S(1)}, f32[2,4]{1,0:T(2,128)}, u32[]{:S(2)}) copy-start(f32[2,4]{1,0:T(2,128)} %param.23) | copy-start | bytes 100
  125.6 64.8 %reduce-scatter.22.cloned.1.call-start = ((), (), s32[]{:S(2)}) async-start(), calls=%async_computation.7 | async-start | bytes 655360
  126.8 87.6 %reduce-scatter.24.cloned.1.call-start = ((), (), s32[]{:S(2)}) async-start(), calls=%async_computation.8 | async-start | bytes 655360
  133.7 86.6 %copy-start.11 = (f32[128]{0:T(128)S(1)}, f32[128]{0:T(128)}, u32[]{:S(2)}) copy-start(f32[128]{0:T(128)} %param.36) | copy-start | bytes 1540
  133.8 111.8 %reduce-scatter.26.cloned.1.call-start = ((), (), s32[]{:S(2)}) async-start(), calls=%async_computation.9 | async-start | bytes 983040
  218.9 0.8 copy-start.3
  220.9 57.0 %copy-start.8 = (f32[768]{0:T(1024)S(1)}, f32[768]{0:T(1024)}, u32[]{:S(2)}) copy-start(f32[768]{0:T(1024)} %param.38) | copy-start | bytes 9220
  222.2 89.4 %all-reduce.8.cloned.1.call-start = ((), (), s32[]{:S(2)}) async-start(), calls=%async_computation.10 | async-start | bytes 148480 | tf_op jit(solution)/shard_map/psum | solution.py:19
  277.2 3.2 copy-start.5
Sparse Core Ops, SparseCore 0:
  44.5 30.7 all-reduce.9
  122.1 19.5 reduce-scatter.17
  144.8 21.5 reduce-scatter.19
  168.7 21.6 reduce-scatter.21
  192.7 21.6 reduce-scatter.23
  222.3 23.2 reduce-scatter.25
  281.7 29.7 all-reduce.7
where the time goes:
time: 360 us; the launch traced here: 359 us
  waiting for transfers between devices  153 us (42%)
  blocking collectives  152 us (42%)
  matrix products  20.1 us (6%)
  between operations  15 us (4%)
  local copies, waits for them, and re-layouts  13.6 us (4%)
  other arithmetic  5.3 us (1%)
    unnamed x12, waiting for transfers between devices  93.2 us
    psum x2, blocking collectives, feed_forward(): whole_sum = lax.psum(down_part, 'kv')  75.8 us
    all_gather x2, blocking collectives, feed_forward(): gathered = lax.all_gather(rows_in, 'kv', axis=0, tiled=True)  63.2 us
    psum x2, waiting for transfers between devices, feed_forward(): lax.psum(lift_part.astype(jnp.bfloat16), 'tp').astype(jnp.float32)  59.4 us
    unnamed x43, local copies, waits for them, and re-layouts  13.5 us
    unnamed x1, blocking collectives  7.82 us
  transfers between devices with their start and end apart: 7, of which 7 were waited for; matrix products, arithmetic and copies ran while one was open for 3% of the time, Pallas kernels for 0%

commit v1 on v0

--- a/solution.py
+++ b/solution.py
@@ -8,7 +8,9 @@
 
 def feed_forward(resid, rows_in, gain, gate_proj, lift_proj, down_proj):
     model_width = gain.shape[0] * lax.axis_size("tp")
-    gathered = lax.all_gather(rows_in, "kv", axis=0, tiled=True)
+    gathered = jnp.concatenate(
+        lax.all_to_all(jnp.stack([rows_in] * lax.axis_size("kv")), "kv", 0, 0), axis=0
+    )
     values = gathered.astype(jnp.float32)
     scaled = (values * gain).astype(jnp.bfloat16)
     gate_part = jnp.dot(scaled, gate_proj, preferred_element_type=jnp.float32)

time: 360 us -> 317 us (0.88)
  blocking collectives: 152 us -> 115 us
  waiting for transfers between devices: 153 us -> 146 us
    all_gather x2 -> x0, blocking collectives: 63.2 us -> none  [feed_forward(): gathered = lax.all_gather(rows_in, 'kv', axis=0, tiled=True)]
    all_to_all x0 -> x2, blocking collectives: none -> 25.8 us  [feed_forward(): lax.all_to_all(jnp.stack([rows_in] * lax.axis_size('kv')), 'kv', 0, 0)]
    psum x2, waiting for transfers between devices: 59.4 us -> 52.5 us  [feed_forward(): lax.psum(lift_part.astype(jnp.bfloat16), 'tp').astype(jnp.float32)]
where the time goes in v1:
time: 317 us; the launch traced here: 316 us
  waiting for transfers between devices  146 us (46%)
  blocking collectives  115 us (36%)
  matrix products  20.3 us (6%)
  local copies, waits for them, and re-layouts  15.7 us (5%)
  between operations  15 us (5%)
  other arithmetic  4.27 us (1%)
    unnamed x12, waiting for transfers between devices  93.2 us
    psum x2, blocking collectives, feed_forward(): whole_sum = lax.psum(down_part, 'kv')  75.8 us
    psum x2, waiting for transfers between devices, feed_forward(): lax.psum(lift_part.astype(jnp.bfloat16), 'tp').astype(jnp.float32)  52.5 us
    all_to_all x2, blocking collectives, feed_forward(): lax.all_to_all(jnp.stack([rows_in] * lax.axis_size('kv')), 'kv', 0, 0)  25.8 us
    unnamed x43, local copies, waits for them, and re-layouts  13.5 us
    unnamed x1, blocking collectives  7.82 us
  transfers between devices with their start and end apart: 7, of which 7 were waited for; matrix products, arithmetic and copies ran while one was open for 3% of the time, Pallas kernels for 0%

profile of v1, /device:TPU:0, one launch (start us, length us, event | category | flops | bytes accessed | tf_op | source)
XLA Modules:
  0.0 316.4 jit_solution(3337487044434063234)
XLA Ops:
  7.2 0.9 stack.4
  8.1 13.9 %all_to_all.10 = bf16[8,2,768]{2,1,0:T(2,128)(2,1)S(1)} all-to-all(bf16[8,2,768]{2,1,0:T(2,128)(2,1)S(1)} %stack.4), channel_id=1, replica_groups=mesh['kv'=8,'tp'=4] {'kv'}, dimensions={0} | all-to-all | bytes 49152 | tf_op jit(solution)/shard_map/all_to_all | solution.py:12
  22.1 0.6 convert_element_type.149
  22.7 2.7 convolution_convert_fusion.3
  25.5 1.2 convolution_convert_fusion.4
  26.8 0.6 dynamic-slice
  28.0 26.0 %all-reduce.10.cloned.1.call-done = (bf16[16,1056]{1,0:T(8,128)(2,1)}, bf16[16,1056]{1,0:T(8,128)(2,1)}, bf16[16]{0:T(256)(128)(2,1)}) async-done(((bf16[16,1056]{1,0:T(8,128)(2,1)}, bf16[16,1056]{1,0:T(8,128)(2,1)}, bf16[16]{0:T(256)(128)(2,1)}), (bf16[16,1056]{1,0:T(8,128)(2,1)}, bf16[16,1056]{1,0:T(8,128)(2,1)}, bf16[16]{0:T(256)(128)(2,1)})) %all-reduce.10.cloned.1.call-update) | async-done | bytes 67632 | tf_op jit(solution)/shard_map/psum | solution.py:21
  54.1 0.7 add_rsqrt_fusion.5
  54.7 1.9 fusion
  56.6 37.9 %psum.66 = bf16[16,768]{1,0:T(8,128)(2,1)S(1)} all-reduce(f32[16,768]{1,0:T(8,128)S(1)} %fusion), channel_id=1, replica_groups=mesh['kv'=8,'tp'=4] {'kv'}, use_global_device_ids=true, to_apply=%region_4.5 | all-reduce | flops 12288 | bytes 73728 | tf_op jit(solution)/shard_map/psum | solution.py:29
  94.5 0.1 multiply_reduce_fusion.2
  94.7 2.6 convolution_convert_fusion.5
  97.2 0.1 copy-done.1
  97.3 0.5 convolution_convert_fusion.6
  97.9 1.4 copy-done.2
  99.2 0.5 convolution_convert_fusion.8
  99.8 1.1 copy.33
  100.9 2.4 convolution_convert_fusion.7
  103.3 1.1 copy.37
  104.5 0.1 convolution_convert_fusion.9
  104.6 1.1 copy.39
  105.9 5.6 %psum.67 = f32[2]{0:T(128)S(1)} all-reduce(f32[2]{0:T(128)S(1)} %get-tuple-element.12), channel_id=1, replica_groups=mesh['kv'=8,'tp'=4] {'tp'}, use_global_device_ids=true, to_apply=%region_6.7 | all-reduce | flops 2 | bytes 16 | tf_op jit(solution)/shard_map/psum | solution.py:71
  111.5 1.1 copy.41
  112.7 7.8 %all-reduce.3 = (bf16[2,16]{1,0:T(2,128)(2,1)S(1)}, bf16[2,16]{1,0:T(2,128)(2,1)S(1)}) all-reduce(bf16[2,16]{1,0:T(2,128)(2,1)S(1)} %convolution_convert_fusion.9, bf16[2,16]{1,0:T(2,128)(2,1)S(1)} %convolution_convert_fusion.10), channel_id=4, replica_groups=mesh['kv'=8,'tp'=4] {'tp'}, use_global_device_ids=true, to_apply=%region_10.11.clone | all-reduce | flops 64 | bytes 256
  120.5 1.0 copy.34
  121.5 23.7 %reduce-scatter.20.cloned.1.call-done = bf16[512,2]{1,0:T(8,128)(2,1)} async-done(((bf16[2048,2]{1,0:T(8,128)(2,1)}), bf16[512,2]{1,0:T(8,128)(2,1)}) %reduce-scatter.20.cloned.1.call-update) | async-done | bytes 2064
  145.2 1.0 copy.38
  146.2 23.0 %reduce-scatter.22.cloned.1.call-done = bf16[512,2]{1,0:T(8,128)(2,1)} async-done(((bf16[2048,2]{1,0:T(8,128)(2,1)}), bf16[512,2]{1,0:T(8,128)(2,1)}) %reduce-scatter.22.cloned.1.call-update) | async-done | bytes 2064
  169.3 1.0 copy.40
  170.3 23.0 %reduce-scatter.24.cloned.1.call-done = bf16[512,2]{1,0:T(8,128)(2,1)} async-done(((bf16[2048,2]{1,0:T(8,128)(2,1)}), bf16[512,2]{1,0:T(8,128)(2,1)}) %reduce-scatter.24.cloned.1.call-update) | async-done | bytes 2064
  193.3 1.0 copy.42
  194.9 1.6 fusion.17
  196.4 1.3 multiply_add_fusion
  197.7 0.8 copy-done.3
  198.5 0.5 fusion.18
  199.2 0.5 convolution_convert_fusion
  199.7 1.2 copy.43
  201.0 23.3 %reduce-scatter.26.cloned.1.call-done = bf16[768,2]{1,0:T(8,128)(2,1)} async-done(((bf16[3072,2]{1,0:T(8,128)(2,1)}), bf16[768,2]{1,0:T(8,128)(2,1)}) %reduce-scatter.26.cloned.1.call-update) | async-done | bytes 3088
  224.3 1.0 copy.44
  225.4 11.9 %all_to_all.11 = bf16[8,2,768]{2,1,0:T(2,128)(2,1)S(1)} all-to-all(bf16[8,2,768]{2,1,0:T(2,128)(2,1)S(1)} %stack.5), channel_id=1, replica_groups=mesh['kv'=8,'tp'=4] {'kv'}, dimensions={0} | all-to-all | bytes 49152 | tf_op jit(solution)/shard_map/all_to_all | solution.py:12
  237.5 0.6 convert_element_type.181
  238.1 2.7 convolution_convert_fusion.1
  240.9 1.2 convolution_convert_fusion.2
  242.0 26.5 %all-reduce.8.cloned.1.call-done = (bf16[16,1056]{1,0:T(8,128)(2,1)}, bf16[16,1056]{1,0:T(8,128)(2,1)}, bf16[16]{0:T(256)(128)(2,1)}) async-done(((bf16[16,1056]{1,0:T(8,128)(2,1)}, bf16[16,1056]{1,0:T(8,128)(2,1)}, bf16[16]{0:T(256)(128)(2,1)}), (bf16[16,1056]{1,0:T(8,128)(2,1)}, bf16[16,1056]{1,0:T(8,128)(2,1)}, bf16[16]{0:T(256)(128)(2,1)})) %all-reduce.8.cloned.1.call-update) | async-done | bytes 67632 | tf_op jit(solution)/shard_map/psum | solution.py:21
  268.5 0.7 add_rsqrt_fusion.3
  269.2 1.9 fusion.1
  271.0 37.9 %psum.71 = bf16[16,768]{1,0:T(8,128)(2,1)S(1)} all-reduce(f32[16,768]{1,0:T(8,128)S(1)} %fusion.1), channel_id=1, replica_groups=mesh['kv'=8,'tp'=4] {'kv'}, use_global_device_ids=true, to_apply=%region_21.22 | all-reduce | flops 12288 | bytes 73728 | tf_op jit(solution)/shard_map/psum | solution.py:29
  308.9 0.6 add_convert_fusion
  (67 shorter events, 1.7 us)
Async XLA Ops:
  7.2 192.0 %copy-start = (bf16[512,3072]{1,0:T(8,128)(2,1)S(1)}, bf16[512,3072]{1,0:T(8,128)(2,1)}, u32[]{:S(2)}) copy-start(bf16[512,3072]{1,0:T(8,128)(2,1)} %param.37) | copy-start | bytes 9437188
  7.2 18.3 %copy-start.7 = (f32[768]{0:T(1024)S(1)}, f32[768]{0:T(1024)}, u32[]{:S(2)}) copy-start(f32[768]{0:T(1024)} %param.25) | copy-start | bytes 9220
  7.2 46.9 %all-reduce.10.cloned.1.call-start = ((), (), s32[]{:S(2)}) async-start(), calls=%async_computation.13 | async-start | bytes 148480 | tf_op jit(solution)/shard_map/psum | solution.py:21
  22.7 2.8 copy-start.4
  22.7 4.0 %copy-start.14 = (f32[4]{0:T(128)S(1)}, f32[4]{0:T(128)}, u32[]{:S(2)}) copy-start(f32[4]{0:T(128)} %param.24) | copy-start | bytes 52
  22.7 4.0 %copy-start.15 = (u32[32]{0:T(128)S(1)}, u32[32]{0:T(128)}, u32[]{:S(2)}) copy-start(u32[32]{0:T(128)} %constant.47) | copy-start | bytes 388
  25.5 69.0 %copy-start.6 = (bf16[2,768]{1,0:T(2,128)(2,1)S(1)}, bf16[2,768]{1,0:T(2,128)(2,1)}, u32[]{:S(2)}) copy-start(bf16[2,768]{1,0:T(2,128)(2,1)} %param.21) | copy-start | bytes 9220
  25.5 69.0 %copy-start.9 = (f32[768]{0:T(1024)S(1)}, f32[768]{0:T(1024)}, u32[]{:S(2)}) copy-start(f32[768]{0:T(1024)} %param.29) | copy-start | bytes 9220
  26.7 93.9 %reduce-scatter.18.cloned.1.call-start = ((), (), s32[]{:S(2)}) async-start(), calls=%async_computation.7 | async-start | bytes 655360
  94.5 2.8 copy-start.1
  97.3 1.9 copy-start.2
  100.9 3.6 %copy-start.12 = (bf16[768,16]{0,1:T(8,128)(2,1)S(1)}, bf16[768,16]{0,1:T(8,128)(2,1)}, u32[]{:S(2)}) copy-start(bf16[768,16]{0,1:T(8,128)(2,1)} %param.34) | copy-start | bytes 73732
  100.9 44.3 %reduce-scatter.20.cloned.1.call-start = ((), (), s32[]{:S(2)}) async-start(), calls=%async_computation.8 | async-start | bytes 655360
  103.3 2.4 copy-start.13
  104.4 90.3 %copy-start.10 = (f32[2,4]{1,0:T(2,128)S(1)}, f32[2,4]{1,0:T(2,128)}, u32[]{:S(2)}) copy-start(f32[2,4]{1,0:T(2,128)} %param.23) | copy-start | bytes 100
  104.4 64.8 %reduce-scatter.22.cloned.1.call-start = ((), (), s32[]{:S(2)}) async-start(), calls=%async_computation.9 | async-start | bytes 655360
  105.7 87.6 %reduce-scatter.24.cloned.1.call-start = ((), (), s32[]{:S(2)}) async-start(), calls=%async_computation.10 | async-start | bytes 655360
  112.6 86.6 %copy-start.11 = (f32[128]{0:T(128)S(1)}, f32[128]{0:T(128)}, u32[]{:S(2)}) copy-start(f32[128]{0:T(128)} %param.36) | copy-start | bytes 1540
  112.6 111.7 %reduce-scatter.26.cloned.1.call-start = ((), (), s32[]{:S(2)}) async-start(), calls=%async_computation.11 | async-start | bytes 983040
  197.7 0.8 copy-start.3
  199.7 38.4 %copy-start.8 = (f32[768]{0:T(1024)S(1)}, f32[768]{0:T(1024)}, u32[]{:S(2)}) copy-start(f32[768]{0:T(1024)} %param.38) | copy-start | bytes 9220
  201.0 67.5 %all-reduce.8.cloned.1.call-start = ((), (), s32[]{:S(2)}) async-start(), calls=%async_computation.12 | async-start | bytes 148480 | tf_op jit(solution)/shard_map/psum | solution.py:21
  238.1 2.7 copy-start.5
Sparse Core Ops, SparseCore 0:
  26.8 27.2 all-reduce.9
  101.0 19.5 reduce-scatter.17
  123.6 21.5 reduce-scatter.19
  147.6 21.6 reduce-scatter.21
  171.6 21.6 reduce-scatter.23
  201.1 23.1 reduce-scatter.25
  242.2 26.3 all-reduce.7
